TPU v7x, 128 devices: a whole 4x4x4 slice. The times are simulated.
128 devices in a mesh: sp: 16 (over z, y), tp: 8 (over x, core).
Axes of the slice: x: 4, y: 4, z: 4, core: 2. Of those that a mesh axis runs over, the one named last changes fastest.
Arguments:
- stream: bfloat16 [32768, 4096], P('sp', 'tp'), may hold values from -18 to 18
- doc_ids: int32 [32768], P('sp'), may hold values from 0 to 3, never falling along the last dimension, each value on 1 to 12288 neighbouring positions
- norm_gain: bfloat16 [3, 4096], replicated, may hold values from 0.099609375 to 1.8984375
- proj_in: bfloat16 [3, 4096, 1024], P(None, 'tp', 'sp'), may hold values from -0.09375 to 0.09375
- mix_pool: bfloat16 [3, 8, 128, 128], replicated, may hold values from -0.5 to 0.5
- pool_gain: bfloat16 [3, 1024], replicated, may hold values from 0.099609375 to 1.8984375
- proj_out: bfloat16 [3, 1024, 4096], P(None, 'sp', 'tp'), may hold values from -0.1875 to 0.1875
Outputs:
- stream_out: bfloat16 [32768, 4096], P('sp', 'tp')
Inputs may be any that keep to these rules, and one draw needn't show every extreme that they name: `doc_ids`: document numbers never fall along the sequence; each document holds 1 to 12288 positions, one exactly that many.
All inputs are finite; a program needn't handle non-finite values.
Results may differ from a plain program's by a relative error of at most 0.02.
Values may be sent and summed in bfloat16 or wider, within the bound.
No kernel may reach another device: no remote copies, remote signals or barrier semaphores. Data moves between devices by JAX's collectives and lax.ppermute only.
A program may use at most 64 MiB of HBM per device.

v0:
```python
import functools

import jax
import jax.numpy as jnp
from jax import lax
from jax.experimental import pallas as pl
from jax.experimental.pallas import tpu as pltpu
from jax.sharding import Mesh, PartitionSpec as P


epsilon = 1e-06
HALO = 64
TAIL = 16
EXTRA = 16
PIECES = 1
VMEM_LIMIT = 16 * 1024 * 1024
LANES = 1024
SEQ = ("z", "y")
F32 = jnp.float32
BF16 = jnp.bfloat16


def nt_dot(a, b):
    return lax.dot_general(a, b, (((1,), (1,)), ((), ())), preferred_element_type=F32)


def dot(a, b):
    return jnp.dot(a, b, preferred_element_type=F32)


def quarter_of(weight, at, index, k):
    return weight[pl.ds(index[k] * 4, 4), at].reshape(256, weight.shape[3])


def call(kernel, operands, shapes, flops, scalars=True, scratch=()):
    memory = pl.BlockSpec(memory_space=pltpu.VMEM)
    specs = [memory] * len(operands)
    if scalars:
        specs[0] = pl.BlockSpec(memory_space=pltpu.SMEM)
    return pl.pallas_call(
        kernel,
        in_specs=specs,
        out_specs=[memory] * len(shapes),
        out_shape=[jax.ShapeDtypeStruct(s, t) for s, t in shapes],
        scratch_shapes=list(scratch),
        compiler_params=pltpu.CompilerParams(vmem_limit_bytes=VMEM_LIMIT),
        cost_estimate=pl.CostEstimate(flops=flops, bytes_accessed=1024, transcendentals=0),
    )(*operands)


def packed(total, lanes):
    high = total.astype(BF16).astype(F32)
    low = total - high
    count = LANES // lanes
    row = lax.broadcasted_iota(jnp.int32, (EXTRA, lanes), 0)
    out = jnp.zeros((EXTRA, lanes), F32)
    for i in range(count):
        cols = slice(i * lanes, (i + 1) * lanes)
        out = jnp.where(row == i, high[:, cols], out)
        out = jnp.where(row == count + i, low[:, cols], out)
    return out.astype(BF16)


def unpacked(block):
    count = LANES // block.shape[1]
    value = block.astype(F32)
    return jnp.concatenate(
        [value[i : i + 1] + value[count + i : count + i + 1] for i in range(count)], axis=1
    )


def square_sums(wide, ones):
    fold = wide * wide
    fold = sum(fold[:, i : i + 128] for i in range(0, fold.shape[1], 128))
    high = fold.astype(BF16)
    low = (fold - high.astype(F32)).astype(BF16)
    return nt_dot(ones, high) + nt_dot(ones, low)


def over_pieces(rows, one):
    size = rows // PIECES
    for i in range(PIECES):
        one(i, slice(i * size, (i + 1) * size))


def project_piece(index, i, here, wide, gain, weight, at, keep, send, sums):
    sums[i] = square_sums(wide, jnp.ones((8, 128), BF16))
    gained = (wide * gain[...]).astype(BF16)
    for k in range(4):
        columns = jnp.concatenate([quarter_of(weight, j, index, k) for j in at], axis=1)
        part = nt_dot(gained, columns)
        out = keep if k < 2 else send
        out[here, (k % 2) * 256 : (k % 2 + 1) * 256] = part.astype(BF16)


def finish_squares(sums, rows, send, squares):
    parts = [sums[i] for i in range(PIECES)]
    total = jnp.concatenate(parts + [jnp.zeros((8, LANES - rows), F32)], axis=1)[0:1]
    send[rows : rows + EXTRA, :] = packed(total, send.shape[1])
    squares[...] = total


def project_body(index, both, gain, weight, keep, send, squares, sums):
    rows = both.shape[1]

    def turn(half, carry):
        wide = both[half].astype(F32)
        project_piece(
            index, 0, slice(0, rows), wide, gain, weight, (0,), keep.at[half], send.at[half], sums
        )
        finish_squares(sums, rows, send.at[half], squares.at[half])
        return carry

    lax.fori_loop(0, 2, turn, 0)


def updated(index, here, parts, old, weight, at):
    total = old[here, :].astype(F32)
    for k, part in enumerate(parts):
        total = total + dot(part[here, :], quarter_of(weight, at, index, k))
    return total.astype(BF16)


def step_body(
    index, m0, m1, m2, m3, own, other, gain, weight, new_own, new_other, keep, send, squares, sums
):
    def one(i, here):
        first = updated(index, here, (m0, m1, m2, m3), own, weight, 0)
        second = updated(index, here, (m0, m1, m2, m3), other, weight, 1)
        new_own[here, :] = first
        new_other[here, :] = second
        wide = jnp.concatenate([first, second], axis=1).astype(F32)
        project_piece(index, i, here, wide, gain, weight, (2, 3), keep, send, sums)

    over_pieces(own.shape[0], one)
    finish_squares(sums, own.shape[0], send, squares)


def last_body(skip, index, m0, m1, m2, m3, own, other, weight, out, out_other):
    here = slice(skip, own.shape[0])
    out[...] = updated(index, here, (m0, m1, m2, m3), own, weight, 0)
    out_other[...] = updated(index, here, (m0, m1, m2, m3), other, weight, 1)


def merge_body(keep, core, squares, partner, chip):
    rows = keep.shape[0]
    partner[:rows, :] = (
        keep[:, 256:].astype(F32) + core[:rows, 256:].astype(F32)
    ).astype(BF16)
    total = squares[...] + unpacked(core[rows : rows + EXTRA, :])
    chip[...] = total
    partner[rows : rows + EXTRA, :] = packed(total, 256)


def scatter_body(keep, core, squares, to_pair, to_flip, to_cross, chip):
    rows = keep.shape[1]
    extra = slice(rows, rows + EXTRA)
    totals = [squares[half] + unpacked(core[half, extra, :]) for half in range(2)]
    chip[...] = totals[0]
    for out, half, first in ((to_pair, 0, 256), (to_flip, 1, 256), (to_cross, 1, 0)):
        cols = slice(first, first + 256)
        out[:rows, :] = (
            keep[half, :, cols].astype(F32) + core[half, :rows, cols].astype(F32)
        ).astype(BF16)
        out[extra, :] = packed(totals[half], 256)


def pool_rows(model_width, first, near, far, across, chip, tail, band, share, mix, gain, mixed, new_tail, scales):
    rows = mixed.shape[0]
    total = chip[...]
    for part in across:
        total = total + unpacked(part[rows : rows + EXTRA, :])
    scale = lax.rsqrt(total * (1.0 / model_width) + epsilon)
    for i in range(LANES // 128):
        scales[i] = scale[:, 128 * i : 128 * i + 128]

    def block(i, size, before):
        at = i * 128
        if looped:
            at = pl.multiple_of(at, 128)
        here, there = pl.ds(at, size), pl.ds(first + at, size)
        turned = jnp.transpose(jnp.broadcast_to(scales[i], (128, 128)))[:size]
        summed = near(here).astype(F32) + far(here).astype(F32)
        for part in across:
            summed = summed + part[here, :].astype(F32)
        z = (summed * jnp.concatenate([turned, turned], axis=1)).astype(BF16)
        window = jnp.concatenate([before, z], axis=0)
        for g in range(2):
            cols = slice(g * 128, (g + 1) * 128)
            sums = dot(band[g, there, : size + TAIL], window[:, cols])
            pooled = (sums * share[g, there, :] - z[:, cols].astype(F32)).astype(BF16)
            blended = dot(pooled, mix[g]) * gain[0:1, cols]
            mixed[here, cols] = blended.astype(BF16)
        return z[size - TAIL :]

    whole = rows // 128
    looped = len(across) > 1 or rows % 128 > 0
    before = tail[...]
    if looped:
        before = lax.fori_loop(0, whole, lambda i, carry: block(i, 128, carry), before)
        looped = False
    else:
        for i in range(whole):
            before = block(i, 128, before)
    if rows > whole * 128:
        before = block(whole, rows - whole * 128, before)
    new_tail[...] = before


def pool_body(model_width, first, near, far, across, *rest):
    pool_rows(
        model_width, first, lambda r: near[r, :256], lambda r: far[r, :256], (across,), *rest
    )


def pool_first_body(model_width, first, near, far, across, flipped, crossed, *rest):
    pool_rows(
        model_width,
        first,
        lambda r: near[0, r, :256],
        lambda r: far[0, r, :256],
        (across, flipped, crossed),
        *rest,
    )


def prepare_body(proj_in, proj_out, opening, mine):
    size = proj_in.shape[2]
    row = lax.broadcasted_iota(jnp.int32, (size, size), 0)
    eye = (row == lax.broadcasted_iota(jnp.int32, (size, size), 1)).astype(BF16)
    opening[...] = nt_dot(eye, proj_in[0]).astype(BF16)
    layers = proj_in.shape[0]
    for layer in range(layers):
        mine[2 * layer] = proj_out[layer]
        if layer + 1 < layers:
            mine[2 * layer + 1] = nt_dot(eye, proj_in[layer + 1]).astype(BF16)


def arrange_body(mine, theirs, out):
    for i in range(mine.shape[0]):
        out[2 * i] = mine[i]
        out[2 * i + 1] = theirs[i]


def along_sequence(value, count):
    return lax.ppermute(value, SEQ, [(i, i + 1) for i in range(count - 1)])


def membership(padded, start, rows, group):
    blocks = -(-rows // 128)
    padded = jnp.pad(padded, (0, 128), constant_values=-1)
    sources = jnp.stack(
        [padded[start + 128 * b : start + 128 * b + 128 + TAIL] for b in range(blocks)]
    )
    targets = padded[start + TAIL : start + TAIL + 128 * blocks].reshape(blocks, 128, 1)
    delta = (
        lax.broadcasted_iota(jnp.int32, (128, 128 + TAIL), 0)
        + TAIL
        - lax.broadcasted_iota(jnp.int32, (128, 128 + TAIL), 1)
    )
    member = (sources[:, None, :] == targets) & (delta >= 0)[None]
    bands, shares = [], []
    for g in range(2):
        window = jnp.left_shift(2, (group + g) % 4)
        band = (member & (delta < window)[None]).reshape(blocks * 128, -1)[:rows]
        count = jnp.sum(band.astype(F32), axis=1, keepdims=True)
        bands.append(band.astype(BF16))
        shares.append(jnp.broadcast_to(1.0 / count, (rows, 128)))
    return jnp.stack(bands), jnp.stack(shares)


def layers_body(stream, doc_ids, norm_gain, proj_in, mix_pool, pool_gain, proj_out):
    layers = proj_in.shape[0]
    tokens, width = stream.shape
    model_width = norm_gain.shape[1]
    places = lax.axis_size(SEQ)
    x, c = lax.axis_index("x"), lax.axis_index("c")
    late, p = x // 2, x % 2
    flip = [(i, 3 - i) for i in range(4)]
    pair = [(i, i ^ 1) for i in range(4)]
    swap = [(0, 1), (1, 0)]
    half = tokens // 2
    rows = half + HALO
    split = half // 2
    streams = [(0, split), (split, rows)]

    shard = (proj_in.shape[2], width)
    opening, mine = call(
        prepare_body,
        (proj_in, proj_out),
        [(shard, BF16), ((2 * layers - 1, *shard), BF16)],
        1024,
        scalars=False,
    )

    def spread(shards):
        return jnp.broadcast_to(shards[None], (places, *shards.shape))

    def everyone(copies):
        return lax.all_to_all(copies, SEQ, 0, 0, tiled=True)

    labels_of = (doc_ids + 1).astype(jnp.int32)
    marks = jnp.pad(
        labels_of[-HALO:].astype(BF16)[None], ((0, EXTRA - 1), (0, width - HALO))
    )
    lead = along_sequence(jnp.concatenate([stream[-HALO:], marks]), places)
    w_first = everyone(spread(opening[None]))
    lead_labels = lead[HALO, :HALO].astype(jnp.int32)
    lead = lead[:HALO]
    middle = stream[half - HALO : half]
    middle_labels = labels_of[half - HALO : half]
    own_lead = jnp.where(late == 1, middle, lead)
    other_lead = jnp.where(late == 1, lead, middle)
    labels = jnp.concatenate(
        [
            jnp.where(late == 1, middle_labels, lead_labels),
            lax.dynamic_slice_in_dim(labels_of, late * half, half),
        ]
    )

    def rows_at(side, s):
        lo, hi = max(0, streams[s][0] - HALO), streams[s][1] - HALO
        return lax.dynamic_slice_in_dim(stream, side * half + lo, hi - lo)

    own = [jnp.concatenate([own_lead, rows_at(late, 0)]), rows_at(late, 1)]
    away = [jnp.concatenate([other_lead, rows_at(1 - late, 0)]), rows_at(1 - late, 1)]
    theirs = lax.ppermute(mine, "x", flip)
    other = []
    for s in range(2):
        other.append(lax.ppermute(away[s], "x", flip))
    arranged = call(
        arrange_body, (mine, theirs), [((4 * layers - 2, *shard), BF16)], 1024, scalars=False
    )[0]
    w_rest = lax.all_gather(arranged, SEQ, axis=0, tiled=False)

    quarters = jnp.stack([2 * c + p, 2 * c + 1 - p, 2 * (1 - c) + p, 2 * (1 - c) + 1 - p]).astype(
        jnp.int32
    )
    group = 2 * (2 * c + p)
    padded = jnp.pad(labels, (TAIL, 0), constant_values=-1)
    band, share = membership(padded, 0, rows, group)

    here, there = (x * 2 + c) * width, ((3 - x) * 2 + c) * width

    def gain_of(layer):
        return jnp.concatenate(
            [lax.dynamic_slice_in_dim(norm_gain[layer], at, width) for at in (here, there)]
        ).astype(F32)[None]

    def sent_shapes(n):
        return [((n, 512), BF16), ((n + EXTRA, 512), BF16), ((1, LANES), F32)]

    def sums_of(n):
        return [pltpu.VMEM((PIECES, 8, n // PIECES), F32)]

    gains = [gain_of(layer) for layer in range(layers)]
    partial, sends = [], []
    for s, (lo, hi) in enumerate(streams):
        n = hi - lo
        partial.append(
            call(
                project_body,
                (quarters, jnp.stack([own[s], away[s]]), gains[0][:, :width], w_first),
                [((2, *shape), kind) for shape, kind in sent_shapes(n)],
                2 * n * 1024 * 1024,
                scratch=sums_of(n),
            )
        )
        sends.append(lax.ppermute(partial[s][1], "c", swap))
    cross = [(i, (i + 2) % 4) for i in range(4)]
    for layer in range(layers):
        mix = lax.dynamic_slice_in_dim(mix_pool[layer], group, 2, 0)
        scale = lax.dynamic_slice_in_dim(pool_gain[layer], group * 128, 256).astype(F32)[None]
        last = layer + 1 == layers
        w_step = w_rest[:, 4 * layer : 4 * layer + 4]
        tail = jnp.zeros((TAIL, 256), BF16)
        merged, parts, back = [], [], []
        for s, (lo, hi) in enumerate(streams):
            n = hi - lo
            keep, _, squares = partial[s]
            message = ((n + EXTRA, 256), BF16)
            routes = (pair, flip, cross) if layer == 0 else (pair,)
            *messages, chip = call(
                scatter_body if layer == 0 else merge_body,
                (keep, sends[s], squares),
                [message] * len(routes) + [((1, LANES), F32)],
                n * 256,
                scalars=False,
            )
            across = [lax.ppermute(value, "x", route) for value, route in zip(messages, routes)]
            merged.append((keep, sends[s], *across, chip))
        for s, (lo, hi) in enumerate(streams):
            n = hi - lo
            mixed, tail = call(
                functools.partial(pool_first_body if layer == 0 else pool_body, model_width, lo),
                (*merged[s], tail, band, share, mix, scale),
                [((n, 256), BF16), ((TAIL, 256), BF16)],
                2 * n * 256 * 1024,
                scalars=False,
                scratch=[pltpu.VMEM((LANES // 128, 1, 128), F32)],
            )
            from_core = lax.ppermute(mixed, "c", swap)
            from_pair = lax.ppermute(mixed, "x", pair)
            from_both = lax.ppermute(from_pair, "c", swap)
            parts.append((mixed, from_pair, from_core, from_both))
        for s, (lo, hi) in enumerate(streams):
            n = hi - lo
            if not last:
                own[s], other[s], *partial[s] = call(
                    step_body,
                    (quarters, *parts[s], own[s], other[s], gains[layer + 1], w_step),
                    [((n, width), BF16)] * 2 + sent_shapes(n),
                    4 * n * 1024 * 1024,
                    scratch=sums_of(n),
                )
            else:
                skip = HALO if s == 0 else 0
                own[s], back_rows = call(
                    functools.partial(last_body, skip),
                    (quarters, *parts[s], own[s], other[s], w_step),
                    [((n - skip, width), BF16)] * 2,
                    2 * n * 1024 * 1024,
                )
            if last:
                back.append(lax.ppermute(back_rows, "x", flip))
            else:
                sends[s] = lax.ppermute(partial[s][1], "c", swap)
    out = jnp.zeros((tokens, width), BF16)
    place = 0
    for s in range(2):
        out = lax.dynamic_update_slice_in_dim(out, own[s], late * half + place, 0)
        out = lax.dynamic_update_slice_in_dim(out, back[s], (1 - late) * half + place, 0)
        place += own[s].shape[0]
    return out


def solution(mesh):
    fine = Mesh(mesh.devices.reshape(4, 4, 4, 2), ("z", "y", "x", "c"))
    sp, tp = ("z", "y"), ("x", "c")
    in_specs = (P(sp, tp), P(sp), P(), P(None, tp, sp), P(), P(), P(None, sp, tp))
    return jax.shard_map(layers_body, mesh=fine, in_specs=in_specs, out_specs=P(sp, tp), check_vma=False)
```

profile of v0, /device:TPU:1, one launch (start us, length us, event | category | flops | bytes accessed | tf_op | source)
XLA Modules:
  0.0 248.0 jit_solution(12405749954406705326)
XLA Ops:
  8.9 3.4 %collective-permute-start.9 = (bf16[5,64,512]{2,1,0:T(8,128)(2,1)S(1)}, bf16[5,64,512]{2,1,0:T(8,128)(2,1)S(1)}, u32[]{:S(2)}, u32[]{:S(2)}) collective-permute-start(bf16[5,64,512]{2,1,0:T(8,128)(2,1)S(1)} %get-tuple-element.71.mine), channel_id=1, source_target_pairs={{0,6},{2,4},{4,2},{6,0},{1,7},{3,5},{5,3},{7,1},{8,14},{10,12},{12... | collective-permute-start | bytes 983048 | tf_op jit(solution)/shard_map/ppermute | solution.py:327
  12.3 7.1 %collective-permute-done.9.theirs = bf16[5,64,512]{2,1,0:T(8,128)(2,1)S(1)} collective-permute-done((bf16[5,64,512]{2,1,0:T(8,128)(2,1)S(1)}, bf16[5,64,512]{2,1,0:T(8,128)(2,1)S(1)}, u32[]{:S(2)}, u32[]{:S(2)}) %collective-permute-start.9) | collective-permute-done | bytes 327712 | tf_op jit(solution)/shard_map/ppermute | solution.py:327
  21.0 4.1 %collective-permute-start = (bf16[80,512]{1,0:T(8,128)(2,1)}, bf16[80,512]{1,0:T(8,128)(2,1)}, u32[]{:S(2)}, u32[]{:S(2)}) collective-permute-start(bf16[80,512]{1,0:T(8,128)(2,1)} %fusion.5), channel_id=1, source_target_pairs={{0,8},{8,16},{16,24},{24,32},{32,40},{40,48},{48,56},{56,64},{64,7... | collective-permute-start | bytes 245768 | tf_op jit(solution)/shard_map/ppermute | solution.py:246
  26.2 7.0 %all-to-all-start = ((bf16[16,1,64,512]{3,2,1,0:T(8,128)(2,1)}), bf16[16,1,64,512]{3,2,1,0:T(8,128)(2,1)S(1)}, u32[]{:S(2)}, u32[]{:S(2)}) async-start(bf16[16,1,64,512]{3,2,1,0:T(8,128)(2,1)} %broadcast_in_dim.8), calls=%async_computation | async-start | bytes 2097152 | tf_op jit(solution)/shard_map/all_to_all | solution.py:300
  44.9 11.6 %all-to-all-done.weight = bf16[16,1,64,512]{3,2,1,0:T(8,128)(2,1)S(1)} async-done(((bf16[16,1,64,512]{3,2,1,0:T(8,128)(2,1)}), bf16[16,1,64,512]{3,2,1,0:T(8,128)(2,1)S(1)}, u32[]{:S(2)}, u32[]{:S(2)}) %all-to-all-start) | async-done | bytes 1048608 | tf_op jit(solution)/shard_map/all_to_all | solution.py:300
  56.5 3.3 %shard_map.74 = (bf16[2,512,512]{2,1,0:T(8,128)(2,1)S(1)}, bf16[2,528,512]{2,1,0:T(8,128)(2,1)}, f32[2,1,1024]{2,1,0:T(1,128)S(1)}) custom-call(s32[4]{0:T(128)S(1)} %pad_add_fusion.1.index, bf16[2,512,512]{2,1,0:T(8,128)(2,1)S(1)} %pad_maximum_fusion.2.both, f32[1,512]{1,0:T(1,128)S(1)} %fusion.6.gain, bf16[16,1,64,512]{3,2,1,0:T(8,128)(2,1)S(1)} %all-to-all-done.weight), custom_call_target="tpu_custom_call" | custom-call | flops 1073741824 | bytes 1024 | tf_op jit(solution)/shard_map/pallas_call | solution.py:40
  60.8 5.2 %collective-permute-start.1 = (bf16[2,528,512]{2,1,0:T(8,128)(2,1)}, bf16[2,528,512]{2,1,0:T(8,128)(2,1)S(1)}, u32[]{:S(2)}, u32[]{:S(2)}) collective-permute-start(bf16[2,528,512]{2,1,0:T(8,128)(2,1)} %get-tuple-element.64), channel_id=1, source_target_pairs={{0,1},{1,0},{2,3},{3,2},{4,5},{5,4},{6,7},{7,6},{8,9},{9,8},{10,11... | collective-permute-start | bytes 3244040 | tf_op jit(solution)/shard_map/ppermute | solution.py:369
  66.0 3.6 %shard_map.85 = (bf16[2,576,512]{2,1,0:T(8,128)(2,1)S(1)}, bf16[2,592,512]{2,1,0:T(8,128)(2,1)}, f32[2,1,1024]{2,1,0:T(1,128)S(1)}) custom-call(s32[4]{0:T(128)S(1)} %pad_add_fusion.1.index, bf16[2,576,512]{2,1,0:T(8,128)(2,1)S(1)} %pad_maximum_fusion.both, f32[1,512]{1,0:T(1,128)S(1)} %fusion.6.gain, bf16[16,1,64,512]{3,2,1,0:T(8,128)(2,1)S(1)} %all-to-all-done.weight), custom_call_target="tpu_custom_call" | custom-call | flops 1207959552 | bytes 1024 | tf_op jit(solution)/shard_map/pallas_call | solution.py:40
  86.7 17.0 %collective-permute-done.4.crossed = bf16[528,256]{1,0:T(8,128)(2,1)S(1)} collective-permute-done((bf16[528,256]{1,0:T(8,128)(2,1)S(1)}, bf16[528,256]{1,0:T(8,128)(2,1)S(1)}, u32[]{:S(2)}, u32[]{:S(2)}) %collective-permute-start.4) | collective-permute-done | bytes 270368 | tf_op jit(solution)/shard_map/ppermute | solution.py:390
  106.6 3.1 %shard_map.87 = (bf16[576,256]{1,0:T(8,128)(2,1)}, bf16[16,256]{1,0:T(8,128)(2,1)}) custom-call(bf16[2,576,512]{2,1,0:T(8,128)(2,1)S(1)} %copy-done.1, bf16[2,592,512]{2,1,0:T(8,128)(2,1)S(1)} %collective-permute-done.21.core.far, bf16[592,256]{1,0:T(8,128)(2,1)S(1)} %collective-permute-done.22.across, bf16[592,256]{1,0:T(8,128)(2,1)S(1)} %collective-permute-done.23.flipped, ...), custom_call_target="tpu_custom_call" | custom-call | flops 301989888 | bytes 1024 | tf_op jit(solution)/shard_map/pallas_call | solution.py:40
  117.4 5.5 %collective-permute-done.5.m1 = bf16[512,256]{1,0:T(8,128)(2,1)} collective-permute-done((bf16[512,256]{1,0:T(8,128)(2,1)}, bf16[512,256]{1,0:T(8,128)(2,1)}, u32[]{:S(2)}, u32[]{:S(2)}) %collective-permute-start.5) | collective-permute-done | bytes 262176 | tf_op jit(solution)/shard_map/ppermute | solution.py:403
  125.4 3.8 %fusion.16 = (bf16[16,4,64,512]{3,2,1,0:T(8,128)(2,1)S(1)}, bf16[16,4,64,512]{3,2,1,0:T(8,128)(2,1)S(1)}) fusion(bf16[16,10,64,512]{3,2,1,0:T(8,128)(2,1)} %bitcast.48), kind=kLoop, calls=%fused_computation.64 | loop fusion | bytes 16777216 | tf_op jit(solution)/shard_map/slice | solution.py:375
  131.9 4.2 %shard_map.88 = (bf16[576,512]{1,0:T(8,128)(2,1)S(1)}, bf16[576,512]{1,0:T(8,128)(2,1)S(1)}, bf16[576,512]{1,0:T(8,128)(2,1)S(1)}, bf16[592,512]{1,0:T(8,128)(2,1)S(1)}, f32[1,1024]{1,0:T(1,128)S(1)}) custom-call(s32[4]{0:T(128)S(1)} %pad_add_fusion.1.index, bf16[576,256]{1,0:T(8,128)(2,1)} %get-tuple-element.98.m0, bf16[576,256]{1,0:T(8,128)(2,1)S(1)} %copy-done.11, ...), custom_call_target="tpu_custom_call" | custom-call | flops 2415919104 | bytes 1024 | tf_op jit(solution)/shard_map/pallas_call | solution.py:40
  136.5 3.9 %shard_map.78 = (bf16[512,512]{1,0:T(8,128)(2,1)S(1)}, bf16[512,512]{1,0:T(8,128)(2,1)S(1)}, bf16[512,512]{1,0:T(8,128)(2,1)S(1)}, bf16[528,512]{1,0:T(8,128)(2,1)S(1)}, f32[1,1024]{1,0:T(1,128)S(1)}) custom-call(s32[4]{0:T(128)S(1)} %pad_add_fusion.1.index, bf16[512,256]{1,0:T(8,128)(2,1)} %get-tuple-element.70.m0, ...), custom_call_target="tpu_custom_call" | custom-call | flops 2147483648 | bytes 1024 | tf_op jit(solution)/shard_map/pallas_call | solution.py:40
  144.1 11.1 %collective-permute-done.11.across = bf16[528,256]{1,0:T(8,128)(2,1)S(1)} collective-permute-done((bf16[528,256]{1,0:T(8,128)(2,1)S(1)}, bf16[528,256]{1,0:T(8,128)(2,1)S(1)}, u32[]{:S(2)}, u32[]{:S(2)}) %collective-permute-start.11) | collective-permute-done | bytes 270368 | tf_op jit(solution)/shard_map/ppermute | solution.py:390
  162.2 4.3 %collective-permute-done.31.m1 = bf16[576,256]{1,0:T(8,128)(2,1)S(1)} collective-permute-done((bf16[576,256]{1,0:T(8,128)(2,1)S(1)}, bf16[576,256]{1,0:T(8,128)(2,1)S(1)}, u32[]{:S(2)}, u32[]{:S(2)}) %collective-permute-start.31) | collective-permute-done | bytes 294944 | tf_op jit(solution)/shard_map/ppermute | solution.py:403
  166.5 3.5 %collective-permute-start.33 = (bf16[576,256]{1,0:T(8,128)(2,1)S(1)}, bf16[576,256]{1,0:T(8,128)(2,1)S(1)}, u32[]{:S(2)}, u32[]{:S(2)}) collective-permute-start(bf16[576,256]{1,0:T(8,128)(2,1)S(1)} %collective-permute-done.31.m1), channel_id=1, source_target_pairs={{0,1},{1,0},{2,3},{3,2},{4,5},{5,4},{6,7},{7,6},{8,9},{9,8},{10,11... | collective-permute-start | bytes 884744 | tf_op jit(solution)/shard_map/ppermute | solution.py:404
  174.1 3.5 %shard_map.91 = (bf16[576,512]{1,0:T(8,128)(2,1)S(1)}, bf16[576,512]{1,0:T(8,128)(2,1)S(1)}, bf16[576,512]{1,0:T(8,128)(2,1)S(1)}, bf16[592,512]{1,0:T(8,128)(2,1)S(1)}, f32[1,1024]{1,0:T(1,128)S(1)}) custom-call(s32[4]{0:T(128)S(1)} %pad_add_fusion.1.index, bf16[576,256]{1,0:T(8,128)(2,1)S(1)} %get-tuple-element.105.m0, ...), custom_call_target="tpu_custom_call" | custom-call | flops 2415919104 | bytes 1024 | tf_op jit(solution)/shard_map/pallas_call | solution.py:40
  178.0 3.2 %shard_map.81 = (bf16[512,512]{1,0:T(8,128)(2,1)S(1)}, bf16[512,512]{1,0:T(8,128)(2,1)S(1)}, bf16[512,512]{1,0:T(8,128)(2,1)S(1)}, bf16[528,512]{1,0:T(8,128)(2,1)S(1)}, f32[1,1024]{1,0:T(1,128)S(1)}) custom-call(s32[4]{0:T(128)S(1)} %pad_add_fusion.1.index, bf16[512,256]{1,0:T(8,128)(2,1)S(1)} %get-tuple-element.77.m0, ...), custom_call_target="tpu_custom_call" | custom-call | flops 2147483648 | bytes 1024 | tf_op jit(solution)/shard_map/pallas_call | solution.py:40
  186.7 4.5 %collective-permute-done.16.across = bf16[528,256]{1,0:T(8,128)(2,1)S(1)} collective-permute-done((bf16[528,256]{1,0:T(8,128)(2,1)S(1)}, bf16[528,256]{1,0:T(8,128)(2,1)S(1)}, u32[]{:S(2)}, u32[]{:S(2)}) %collective-permute-start.16) | collective-permute-done | bytes 270368 | tf_op jit(solution)/shard_map/ppermute | solution.py:390
  192.4 5.3 %collective-permute-done.35.across = bf16[592,256]{1,0:T(8,128)(2,1)S(1)} collective-permute-done((bf16[592,256]{1,0:T(8,128)(2,1)S(1)}, bf16[592,256]{1,0:T(8,128)(2,1)S(1)}, u32[]{:S(2)}, u32[]{:S(2)}) %collective-permute-start.35) | collective-permute-done | bytes 303136 | tf_op jit(solution)/shard_map/ppermute | solution.py:390
  205.3 3.6 %collective-permute-done.36.m1 = bf16[576,256]{1,0:T(8,128)(2,1)S(1)} collective-permute-done((bf16[576,256]{1,0:T(8,128)(2,1)S(1)}, bf16[576,256]{1,0:T(8,128)(2,1)S(1)}, u32[]{:S(2)}, u32[]{:S(2)}) %collective-permute-start.36) | collective-permute-done | bytes 294944 | tf_op jit(solution)/shard_map/ppermute | solution.py:403
  219.2 8.4 %collective-permute-done.20 = bf16[448,512]{1,0:T(8,128)(2,1)S(1)} collective-permute-done((bf16[448,512]{1,0:T(8,128)(2,1)S(1)}, bf16[448,512]{1,0:T(8,128)(2,1)S(1)}, u32[]{:S(2)}, u32[]{:S(2)}) %collective-permute-start.20) | collective-permute-done | bytes 458784 | tf_op jit(solution)/shard_map/ppermute | solution.py:425
  227.7 12.5 %collective-permute-done.39 = bf16[576,512]{1,0:T(8,128)(2,1)S(1)} collective-permute-done((bf16[576,512]{1,0:T(8,128)(2,1)S(1)}, bf16[576,512]{1,0:T(8,128)(2,1)S(1)}, u32[]{:S(2)}, u32[]{:S(2)}) %collective-permute-start.39) | collective-permute-done | bytes 589856 | tf_op jit(solution)/shard_map/ppermute | solution.py:425
  (184 shorter events, 91.1 us)
Async XLA Ops:
  6.5 118.8 %all-gather.3.cloned.1.call-start = ((), (), s32[]{:S(2)}) async-start(), calls=%async_computation.1 | async-start | bytes 11141120 | tf_op jit(solution)/shard_map/all_gather | solution.py:334
  21.0 19.6 %collective-permute-start = (bf16[80,512]{1,0:T(8,128)(2,1)}, bf16[80,512]{1,0:T(8,128)(2,1)}, u32[]{:S(2)}, u32[]{:S(2)}) collective-permute-start(bf16[80,512]{1,0:T(8,128)(2,1)} %fusion.5), channel_id=1, source_target_pairs={{0,8},{8,16},{16,24},{24,32},{32,40},{40,48},{48,56},{56,64},{64,7... | collective-permute-start | bytes 245768 | tf_op jit(solution)/shard_map/ppermute | solution.py:246
  26.2 30.3 %all-to-all-start = ((bf16[16,1,64,512]{3,2,1,0:T(8,128)(2,1)}), bf16[16,1,64,512]{3,2,1,0:T(8,128)(2,1)S(1)}, u32[]{:S(2)}, u32[]{:S(2)}) async-start(bf16[16,1,64,512]{3,2,1,0:T(8,128)(2,1)} %broadcast_in_dim.8), calls=%async_computation | async-start | bytes 2097152 | tf_op jit(solution)/shard_map/all_to_all | solution.py:300
  60.8 12.5 %collective-permute-start.1 = (bf16[2,528,512]{2,1,0:T(8,128)(2,1)}, bf16[2,528,512]{2,1,0:T(8,128)(2,1)S(1)}, u32[]{:S(2)}, u32[]{:S(2)}) collective-permute-start(bf16[2,528,512]{2,1,0:T(8,128)(2,1)} %get-tuple-element.64), channel_id=1, source_target_pairs={{0,1},{1,0},{2,3},{3,2},{4,5},{5,4},{6,7},{7,6},{8,9},{9,8},{10,11... | collective-permute-start | bytes 3244040 | tf_op jit(solution)/shard_map/ppermute | solution.py:369
  78.6 28.0 %collective-permute-start.22 = (bf16[592,256]{1,0:T(8,128)(2,1)S(1)}, bf16[592,256]{1,0:T(8,128)(2,1)S(1)}, u32[]{:S(2)}, u32[]{:S(2)}) collective-permute-start(bf16[592,256]{1,0:T(8,128)(2,1)S(1)} %get-tuple-element.93), channel_id=1, source_target_pairs={{0,2},{2,0},{4,6},{6,4},{1,3},{3,1},{5,7},{7,5},{8,10},{10,8},{12,... | collective-permute-start | bytes 909320 | tf_op jit(solution)/shard_map/ppermute | solution.py:390
  79.4 27.2 %collective-permute-start.23 = (bf16[592,256]{1,0:T(8,128)(2,1)S(1)}, bf16[592,256]{1,0:T(8,128)(2,1)S(1)}, u32[]{:S(2)}, u32[]{:S(2)}) collective-permute-start(bf16[592,256]{1,0:T(8,128)(2,1)S(1)} %get-tuple-element.94), channel_id=1, source_target_pairs={{0,6},{2,4},{4,2},{6,0},{1,7},{3,5},{5,3},{7,1},{8,14},{10,12},{12... | collective-permute-start | bytes 909320 | tf_op jit(solution)/shard_map/ppermute | solution.py:390
  80.0 26.6 %collective-permute-start.24 = (bf16[592,256]{1,0:T(8,128)(2,1)S(1)}, bf16[592,256]{1,0:T(8,128)(2,1)S(1)}, u32[]{:S(2)}, u32[]{:S(2)}) collective-permute-start(bf16[592,256]{1,0:T(8,128)(2,1)S(1)} %get-tuple-element.95), channel_id=1, source_target_pairs={{0,4},{2,6},{4,0},{6,2},{1,5},{3,7},{5,1},{7,3},{8,12},{10,14},{12... | collective-permute-start | bytes 909320 | tf_op jit(solution)/shard_map/ppermute | solution.py:390
  82.9 32.5 %collective-permute-start.28 = (bf16[576,512]{1,0:T(8,128)(2,1)}, bf16[576,512]{1,0:T(8,128)(2,1)}, u32[]{:S(2)}, u32[]{:S(2)}) collective-permute-start(bf16[576,512]{1,0:T(8,128)(2,1)} %get-tuple-element.126), channel_id=1, source_target_pairs={{0,6},{2,4},{4,2},{6,0},{1,7},{3,5},{5,3},{7,1},{8,14},{10,12},{12... | collective-permute-start | bytes 1769480 | tf_op jit(solution)/shard_map/ppermute | solution.py:330
  85.3 18.4 %collective-permute-start.4 = (bf16[528,256]{1,0:T(8,128)(2,1)S(1)}, bf16[528,256]{1,0:T(8,128)(2,1)S(1)}, u32[]{:S(2)}, u32[]{:S(2)}) collective-permute-start(bf16[528,256]{1,0:T(8,128)(2,1)S(1)} %get-tuple-element.68), channel_id=1, source_target_pairs={{0,4},{2,6},{4,0},{6,2},{1,5},{3,7},{5,1},{7,3},{8,12},{10,14},{12... | collective-permute-start | bytes 811016 | tf_op jit(solution)/shard_map/ppermute | solution.py:390
  109.8 15.4 %collective-permute-start.25 = (bf16[576,256]{1,0:T(8,128)(2,1)}, bf16[576,256]{1,0:T(8,128)(2,1)S(1)}, u32[]{:S(2)}, u32[]{:S(2)}) collective-permute-start(bf16[576,256]{1,0:T(8,128)(2,1)} %get-tuple-element.98.m0), channel_id=1, source_target_pairs={{0,2},{2,0},{4,6},{6,4},{1,3},{3,1},{5,7},{7,5},{8,10},{10,8},{12,... | collective-permute-start | bytes 884744 | tf_op jit(solution)/shard_map/ppermute | solution.py:403
  109.8 13.1 %collective-permute-start.5 = (bf16[512,256]{1,0:T(8,128)(2,1)}, bf16[512,256]{1,0:T(8,128)(2,1)}, u32[]{:S(2)}, u32[]{:S(2)}) collective-permute-start(bf16[512,256]{1,0:T(8,128)(2,1)} %get-tuple-element.70.m0), channel_id=1, source_target_pairs={{0,2},{2,0},{4,6},{6,4},{1,3},{3,1},{5,7},{7,5},{8,10},{10,8},{12,... | collective-permute-start | bytes 786440 | tf_op jit(solution)/shard_map/ppermute | solution.py:403
  111.9 24.6 %collective-permute-start.8 = (bf16[512,512]{1,0:T(8,128)(2,1)}, bf16[512,512]{1,0:T(8,128)(2,1)S(1)}, u32[]{:S(2)}, u32[]{:S(2)}) collective-permute-start(bf16[512,512]{1,0:T(8,128)(2,1)} %get-tuple-element.132), channel_id=1, source_target_pairs={{0,6},{2,4},{4,2},{6,0},{1,7},{3,5},{5,3},{7,1},{8,14},{10,12},{12... | collective-permute-start | bytes 1572872 | tf_op jit(solution)/shard_map/ppermute | solution.py:330
  112.3 24.2 %collective-permute-start.6 = (bf16[512,256]{1,0:T(8,128)(2,1)}, bf16[512,256]{1,0:T(8,128)(2,1)}, u32[]{:S(2)}, u32[]{:S(2)}) collective-permute-start(bf16[512,256]{1,0:T(8,128)(2,1)} %get-tuple-element.70.m0), channel_id=1, source_target_pairs={{0,1},{1,0},{2,3},{3,2},{4,5},{5,4},{6,7},{7,6},{8,9},{9,8},{10,11... | collective-permute-start | bytes 786440 | tf_op jit(solution)/shard_map/ppermute | solution.py:402
  115.4 13.9 %collective-permute-start.26 = (bf16[576,256]{1,0:T(8,128)(2,1)}, bf16[576,256]{1,0:T(8,128)(2,1)S(1)}, u32[]{:S(2)}, u32[]{:S(2)}) collective-permute-start(bf16[576,256]{1,0:T(8,128)(2,1)} %get-tuple-element.98.m0), channel_id=1, source_target_pairs={{0,1},{1,0},{2,3},{3,2},{4,5},{5,4},{6,7},{7,6},{8,9},{9,8},{10,11... | collective-permute-start | bytes 884744 | tf_op jit(solution)/shard_map/ppermute | solution.py:402
  122.8 13.7 %collective-permute-start.7 = (bf16[512,256]{1,0:T(8,128)(2,1)}, bf16[512,256]{1,0:T(8,128)(2,1)}, u32[]{:S(2)}, u32[]{:S(2)}) collective-permute-start(bf16[512,256]{1,0:T(8,128)(2,1)} %collective-permute-done.5.m1), channel_id=1, source_target_pairs={{0,1},{1,0},{2,3},{3,2},{4,5},{5,4},{6,7},{7,6},{8,9},{9,8},{10,11... | collective-permute-start | bytes 786440 | tf_op jit(solution)/shard_map/ppermute | solution.py:404
  140.8 15.5 %collective-permute-start.30 = (bf16[592,256]{1,0:T(8,128)(2,1)S(1)}, bf16[592,256]{1,0:T(8,128)(2,1)S(1)}, u32[]{:S(2)}, u32[]{:S(2)}) collective-permute-start(bf16[592,256]{1,0:T(8,128)(2,1)S(1)} %get-tuple-element.102), channel_id=1, source_target_pairs={{0,2},{2,0},{4,6},{6,4},{1,3},{3,1},{5,7},{7,5},{8,10},{10,8},{12,... | collective-permute-start | bytes 909320 | tf_op jit(solution)/shard_map/ppermute | solution.py:390
  142.5 12.7 %collective-permute-start.11 = (bf16[528,256]{1,0:T(8,128)(2,1)S(1)}, bf16[528,256]{1,0:T(8,128)(2,1)S(1)}, u32[]{:S(2)}, u32[]{:S(2)}) collective-permute-start(bf16[528,256]{1,0:T(8,128)(2,1)S(1)} %get-tuple-element.75), channel_id=1, source_target_pairs={{0,2},{2,0},{4,6},{6,4},{1,3},{3,1},{5,7},{7,5},{8,10},{10,8},{12,... | collective-permute-start | bytes 811016 | tf_op jit(solution)/shard_map/ppermute | solution.py:390
  159.1 13.1 %collective-permute-start.12 = (bf16[512,256]{1,0:T(8,128)(2,1)S(1)}, bf16[512,256]{1,0:T(8,128)(2,1)S(1)}, u32[]{:S(2)}, u32[]{:S(2)}) collective-permute-start(bf16[512,256]{1,0:T(8,128)(2,1)S(1)} %get-tuple-element.77.m0), channel_id=1, source_target_pairs={{0,2},{2,0},{4,6},{6,4},{1,3},{3,1},{5,7},{7,5},{8,10},{10,8},{12,... | collective-permute-start | bytes 786440 | tf_op jit(solution)/shard_map/ppermute | solution.py:403
  160.5 13.6 %collective-permute-start.32 = (bf16[576,256]{1,0:T(8,128)(2,1)S(1)}, bf16[576,256]{1,0:T(8,128)(2,1)S(1)}, u32[]{:S(2)}, u32[]{:S(2)}) collective-permute-start(bf16[576,256]{1,0:T(8,128)(2,1)S(1)} %get-tuple-element.105.m0), channel_id=1, source_target_pairs={{0,1},{1,0},{2,3},{3,2},{4,5},{5,4},{6,7},{7,6},{8,9},{9,8},{10,11... | collective-permute-start | bytes 884744 | tf_op jit(solution)/shard_map/ppermute | solution.py:402
  183.6 14.0 %collective-permute-start.35 = (bf16[592,256]{1,0:T(8,128)(2,1)S(1)}, bf16[592,256]{1,0:T(8,128)(2,1)S(1)}, u32[]{:S(2)}, u32[]{:S(2)}) collective-permute-start(bf16[592,256]{1,0:T(8,128)(2,1)S(1)} %get-tuple-element.111), channel_id=1, source_target_pairs={{0,2},{2,0},{4,6},{6,4},{1,3},{3,1},{5,7},{7,5},{8,10},{10,8},{12,... | collective-permute-start | bytes 909320 | tf_op jit(solution)/shard_map/ppermute | solution.py:390
  192.3 11.0 %collective-permute-start.17 = (bf16[512,256]{1,0:T(8,128)(2,1)S(1)}, bf16[512,256]{1,0:T(8,128)(2,1)S(1)}, u32[]{:S(2)}, u32[]{:S(2)}) collective-permute-start(bf16[512,256]{1,0:T(8,128)(2,1)S(1)} %get-tuple-element.85.m0), channel_id=1, source_target_pairs={{0,2},{2,0},{4,6},{6,4},{1,3},{3,1},{5,7},{7,5},{8,10},{10,8},{12,... | collective-permute-start | bytes 786440 | tf_op jit(solution)/shard_map/ppermute | solution.py:403
  200.4 12.1 %collective-permute-start.18 = (bf16[512,256]{1,0:T(8,128)(2,1)S(1)}, bf16[512,256]{1,0:T(8,128)(2,1)S(1)}, u32[]{:S(2)}, u32[]{:S(2)}) collective-permute-start(bf16[512,256]{1,0:T(8,128)(2,1)S(1)} %get-tuple-element.85.m0), channel_id=1, source_target_pairs={{0,1},{1,0},{2,3},{3,2},{4,5},{5,4},{6,7},{7,6},{8,9},{9,8},{10,11... | collective-permute-start | bytes 786440 | tf_op jit(solution)/shard_map/ppermute | solution.py:402
  214.3 13.4 %collective-permute-start.20 = (bf16[448,512]{1,0:T(8,128)(2,1)S(1)}, bf16[448,512]{1,0:T(8,128)(2,1)S(1)}, u32[]{:S(2)}, u32[]{:S(2)}) collective-permute-start(bf16[448,512]{1,0:T(8,128)(2,1)S(1)} %get-tuple-element.89), channel_id=1, source_target_pairs={{0,6},{2,4},{4,2},{6,0},{1,7},{3,5},{5,3},{7,1},{8,14},{10,12},{12... | collective-permute-start | bytes 1376264 | tf_op jit(solution)/shard_map/ppermute | solution.py:425
  216.5 23.7 %collective-permute-start.39 = (bf16[576,512]{1,0:T(8,128)(2,1)S(1)}, bf16[576,512]{1,0:T(8,128)(2,1)S(1)}, u32[]{:S(2)}, u32[]{:S(2)}) collective-permute-start(bf16[576,512]{1,0:T(8,128)(2,1)S(1)} %get-tuple-element.118), channel_id=1, source_target_pairs={{0,6},{2,4},{4,2},{6,0},{1,7},{3,5},{5,3},{7,1},{8,14},{10,12},{12... | collective-permute-start | bytes 1769480 | tf_op jit(solution)/shard_map/ppermute | solution.py:425
  (41 other events, 293.3 us)
Sparse Core Ops, SparseCore 0:
  20.4 92.3 all-gather.2
where the time goes:
time: 249 us; the launch traced here: 248 us
  waiting for transfers between devices  98.4 us (40%)
  starting transfers between devices  58.7 us (24%)
  Pallas kernels  41 us (16%)
  local copies, waits for them, and re-layouts  25.7 us (10%)
  between operations  14 us (6%)
  other arithmetic  10 us (4%)
    pallas_call x22, Pallas kernels, call(): pl.pallas_call(kernel, in_specs=specs, out_specs=[memory] * len(shapes),...  41 us
    ppermute x10, waiting for transfers between devices, layers_body(): lax.ppermute(value, 'x', route)  39 us
    ppermute x2, waiting for transfers between devices, layers_body(): back.append(lax.ppermute(back_rows, 'x', flip))  20.9 us
    ppermute x6, waiting for transfers between devices, layers_body(): from_pair = lax.ppermute(mixed, 'x', pair)  16 us
    ppermute x6, starting transfers between devices, layers_body(): from_both = lax.ppermute(from_pair, 'c', swap)  12 us
    all_to_all x1, waiting for transfers between devices, everyone(): return lax.all_to_all(copies, SEQ, 0, 0, tiled=True)  11.6 us
    ppermute x10, starting transfers between devices, layers_body(): lax.ppermute(value, 'x', route)  8.61 us
    unnamed x45, local copies, waits for them, and re-layouts  8.48 us
  transfers between devices with their start and end apart: 42, of which 17 were waited for; matrix products, arithmetic and copies ran while one was open for 11% of the time, Pallas kernels for 15%

commit v1 on v0

--- a/solution.py
+++ b/solution.py
@@ -28,8 +28,8 @@
     return jnp.dot(a, b, preferred_element_type=F32)
 
 
-def quarter_of(weight, at, index, k):
-    return weight[pl.ds(index[k] * 4, 4), at].reshape(256, weight.shape[3])
+def quarter_of(weight, index, k):
+    return weight[pl.ds(index[k] * 4, 4)].reshape(256, weight.shape[2])
 
 
 def call(kernel, operands, shapes, flops, scalars=True, scratch=()):
@@ -83,11 +83,11 @@
         one(i, slice(i * size, (i + 1) * size))
 
 
-def project_piece(index, i, here, wide, gain, weight, at, keep, send, sums):
+def project_piece(index, i, here, wide, gain, weights, keep, send, sums):
     sums[i] = square_sums(wide, jnp.ones((8, 128), BF16))
     gained = (wide * gain[...]).astype(BF16)
     for k in range(4):
-        columns = jnp.concatenate([quarter_of(weight, j, index, k) for j in at], axis=1)
+        columns = jnp.concatenate([quarter_of(weight, index, k) for weight in weights], axis=1)
         part = nt_dot(gained, columns)
         out = keep if k < 2 else send
         out[here, (k % 2) * 256 : (k % 2 + 1) * 256] = part.astype(BF16)
@@ -106,7 +106,7 @@
     def turn(half, carry):
         wide = both[half].astype(F32)
         project_piece(
-            index, 0, slice(0, rows), wide, gain, weight, (0,), keep.at[half], send.at[half], sums
+            index, 0, slice(0, rows), wide, gain, (weight,), keep.at[half], send.at[half], sums
         )
         finish_squares(sums, rows, send.at[half], squares.at[half])
         return carry
@@ -114,32 +114,32 @@
     lax.fori_loop(0, 2, turn, 0)
 
 
-def updated(index, here, parts, old, weight, at):
+def updated(index, here, parts, old, weight):
     total = old[here, :].astype(F32)
     for k, part in enumerate(parts):
-        total = total + dot(part[here, :], quarter_of(weight, at, index, k))
+        total = total + dot(part[here, :], quarter_of(weight, index, k))
     return total.astype(BF16)
 
 
 def step_body(
-    index, m0, m1, m2, m3, own, other, gain, weight, new_own, new_other, keep, send, squares, sums
+    index, m0, m1, m2, m3, own, other, gain, w0, w1, w2, w3, new_own, new_other, keep, send, squares, sums
 ):
     def one(i, here):
-        first = updated(index, here, (m0, m1, m2, m3), own, weight, 0)
-        second = updated(index, here, (m0, m1, m2, m3), other, weight, 1)
+        first = updated(index, here, (m0, m1, m2, m3), own, w0)
+        second = updated(index, here, (m0, m1, m2, m3), other, w1)
         new_own[here, :] = first
         new_other[here, :] = second
         wide = jnp.concatenate([first, second], axis=1).astype(F32)
-        project_piece(index, i, here, wide, gain, weight, (2, 3), keep, send, sums)
+        project_piece(index, i, here, wide, gain, (w2, w3), keep, send, sums)
 
     over_pieces(own.shape[0], one)
     finish_squares(sums, own.shape[0], send, squares)
 
 
-def last_body(skip, index, m0, m1, m2, m3, own, other, weight, out, out_other):
+def last_body(skip, index, m0, m1, m2, m3, own, other, w0, w1, out, out_other):
     here = slice(skip, own.shape[0])
-    out[...] = updated(index, here, (m0, m1, m2, m3), own, weight, 0)
-    out_other[...] = updated(index, here, (m0, m1, m2, m3), other, weight, 1)
+    out[...] = updated(index, here, (m0, m1, m2, m3), own, w0)
+    out_other[...] = updated(index, here, (m0, m1, m2, m3), other, w1)
 
 
 def merge_body(keep, core, squares, partner, chip):
@@ -237,9 +237,12 @@
 
 
 def arrange_body(mine, theirs, out):
-    for i in range(mine.shape[0]):
+    paired = theirs.shape[0]
+    for i in range(paired):
         out[2 * i] = mine[i]
         out[2 * i + 1] = theirs[i]
+    for i in range(paired, mine.shape[0]):
+        out[paired + i] = mine[i]
 
 
 def along_sequence(value, count):
@@ -304,7 +307,7 @@
         labels_of[-HALO:].astype(BF16)[None], ((0, EXTRA - 1), (0, width - HALO))
     )
     lead = along_sequence(jnp.concatenate([stream[-HALO:], marks]), places)
-    w_first = everyone(spread(opening[None]))
+    w_first = everyone(spread(opening))
     lead_labels = lead[HALO, :HALO].astype(jnp.int32)
     lead = lead[:HALO]
     middle = stream[half - HALO : half]
@@ -324,13 +327,11 @@
 
     own = [jnp.concatenate([own_lead, rows_at(late, 0)]), rows_at(late, 1)]
     away = [jnp.concatenate([other_lead, rows_at(1 - late, 0)]), rows_at(1 - late, 1)]
-    theirs = lax.ppermute(mine, "x", flip)
+    theirs = lax.ppermute(mine[:3], "x", flip)
     other = []
     for s in range(2):
         other.append(lax.ppermute(away[s], "x", flip))
-    arranged = call(
-        arrange_body, (mine, theirs), [((4 * layers - 2, *shard), BF16)], 1024, scalars=False
-    )[0]
+    arranged = call(arrange_body, (mine, theirs), [((8, *shard), BF16)], 1024, scalars=False)[0]
     w_rest = lax.all_gather(arranged, SEQ, axis=0, tiled=False)
 
     quarters = jnp.stack([2 * c + p, 2 * c + 1 - p, 2 * (1 - c) + p, 2 * (1 - c) + 1 - p]).astype(
@@ -372,7 +373,13 @@
         mix = lax.dynamic_slice_in_dim(mix_pool[layer], group, 2, 0)
         scale = lax.dynamic_slice_in_dim(pool_gain[layer], group * 128, 256).astype(F32)[None]
         last = layer + 1 == layers
-        w_step = w_rest[:, 4 * layer : 4 * layer + 4]
+        if layer == 0:
+            *w_step, in_own = [w_rest[:, i] for i in (0, 1, 2, 3, 6)]
+            in_flipped = lax.ppermute(in_own, "x", flip)
+        elif layer == 1:
+            w_step = [*later[:2], in_own, in_flipped]
+        else:
+            w_step = [later[2], out_flipped]
         tail = jnp.zeros((TAIL, 256), BF16)
         merged, parts, back = [], [], []
         for s, (lo, hi) in enumerate(streams):
@@ -408,7 +415,7 @@
             if not last:
                 own[s], other[s], *partial[s] = call(
                     step_body,
-                    (quarters, *parts[s], own[s], other[s], gains[layer + 1], w_step),
+                    (quarters, *parts[s], own[s], other[s], gains[layer + 1], *w_step),
                     [((n, width), BF16)] * 2 + sent_shapes(n),
                     4 * n * 1024 * 1024,
                     scratch=sums_of(n),
@@ -417,10 +424,14 @@
                 skip = HALO if s == 0 else 0
                 own[s], back_rows = call(
                     functools.partial(last_body, skip),
-                    (quarters, *parts[s], own[s], other[s], w_step),
+                    (quarters, *parts[s], own[s], other[s], *w_step),
                     [((n - skip, width), BF16)] * 2,
                     2 * n * 1024 * 1024,
                 )
+            if layer + s == 0:
+                w_rest, own[0] = lax.optimization_barrier((w_rest, own[0]))
+                later = [w_rest[:, i] for i in (4, 5, 7)]
+                out_flipped = lax.ppermute(later[2], "x", flip)
             if last:
                 back.append(lax.ppermute(back_rows, "x", flip))
             else:

time: 249 us -> 239 us (0.960)
  waiting for transfers between devices: 98.4 us -> 91.3 us
  local copies, waits for them, and re-layouts: 25.7 us -> 21.5 us
    all_to_all x1, waiting for transfers between devices: 11.6 us -> 0.01 us  [everyone(): return lax.all_to_all(copies, SEQ, 0, 0, tiled=True)]
    slice x2 -> x1, local copies, waits for them, and re-layouts: 5.58 us -> 0.02 us  [layers_body(): theirs = lax.ppermute(mine[:3], 'x', flip)]
    squeeze x0 -> x2, local copies, waits for them, and re-layouts: none -> 5.26 us  [the longest x1 3.2 us: layers_body(): *w_step, in_own = [w_rest[:, i] for i in (0, 1, 2, 3, 6)]]
    ppermute x1, waiting for transfers between devices: 0.01 us -> 4.74 us  [along_sequence(): return lax.ppermute(value, SEQ, [(i, i + 1) for i in range(count - 1)])]
    unnamed x45 -> x35, local copies, waits for them, and re-layouts: 8.48 us -> 4.61 us
    ppermute x1 -> x3, waiting for transfers between devices: 7.05 us -> 4.25 us  [the longest x1 4.24 us: layers_body(): theirs = lax.ppermute(mine[:3], 'x', flip)]
    ppermute x1 -> x3, starting transfers between devices: 3.38 us -> 6.17 us  [the longest x1 3.38 us: layers_body(): theirs = lax.ppermute(mine[:3], 'x', flip)]
    ppermute x6, starting transfers between devices: 12 us -> 9.27 us  [layers_body(): from_both = lax.ppermute(from_pair, 'c', swap)]
  transfers between devices with their start and end apart: 42 -> 44, of which waited for: 17 -> 16; matrix products, arithmetic and copies ran while one was open for 11% -> 11% of each run, Pallas kernels for 15% -> 16%
where the time goes in v1:
time: 239 us; the launch traced here: 236 us
  waiting for transfers between devices  91.3 us (38%)
  starting transfers between devices  59.6 us (25%)
  Pallas kernels  39.9 us (17%)
  local copies, waits for them, and re-layouts  21.5 us (9%)
  between operations  13.9 us (6%)
  other arithmetic  10.2 us (4%)
    pallas_call x22, Pallas kernels, call(): pl.pallas_call(kernel, in_specs=specs, out_specs=[memory] * len(shapes),...  39.9 us
    ppermute x10, waiting for transfers between devices, layers_body(): lax.ppermute(value, 'x', route)  39.3 us
    ppermute x2, waiting for transfers between devices, layers_body(): back.append(lax.ppermute(back_rows, 'x', flip))  20.9 us
    ppermute x6, waiting for transfers between devices, layers_body(): from_pair = lax.ppermute(mixed, 'x', pair)  18.7 us
    ppermute x6, starting transfers between devices, layers_body(): from_both = lax.ppermute(from_pair, 'c', swap)  9.27 us
    ppermute x10, starting transfers between devices, layers_body(): lax.ppermute(value, 'x', route)  8.66 us
    all_to_all x1, starting transfers between devices, everyone(): return lax.all_to_all(copies, SEQ, 0, 0, tiled=True)  8.17 us
    ppermute x6, starting transfers between devices, layers_body(): from_core = lax.ppermute(mixed, 'c', swap)  7.51 us
  transfers between devices with their start and end apart: 44, of which 16 were waited for; matrix products, arithmetic and copies ran while one was open for 11% of the time, Pallas kernels for 16%

profile of v1, /device:TPU:1, one launch (start us, length us, event | category | flops | bytes accessed | tf_op | source)
XLA Modules:
  0.0 236.4 jit_solution(2478851847749390596)
XLA Ops:
  8.9 3.4 %collective-permute-start.9 = (bf16[3,64,512]{2,1,0:T(8,128)(2,1)S(1)}, bf16[3,64,512]{2,1,0:T(8,128)(2,1)S(1)}, u32[]{:S(2)}, u32[]{:S(2)}) collective-permute-start(bf16[3,64,512]{2,1,0:T(8,128)(2,1)S(1)} %slice.161), channel_id=1, source_target_pairs={{0,6},{2,4},{4,2},{6,0},{1,7},{3,5},{5,3},{7,1},{8,14},{10,12},{12... | collective-permute-start | bytes 589832 | tf_op jit(solution)/shard_map/ppermute | solution.py:330
  12.3 4.2 %collective-permute-done.9.theirs = bf16[3,64,512]{2,1,0:T(8,128)(2,1)S(1)} collective-permute-done((bf16[3,64,512]{2,1,0:T(8,128)(2,1)S(1)}, bf16[3,64,512]{2,1,0:T(8,128)(2,1)S(1)}, u32[]{:S(2)}, u32[]{:S(2)}) %collective-permute-start.9) | collective-permute-done | bytes 196640 | tf_op jit(solution)/shard_map/ppermute | solution.py:330
  18.5 8.2 %all-to-all-start = ((bf16[16,64,512]{2,1,0:T(8,128)(2,1)}), bf16[16,64,512]{2,1,0:T(8,128)(2,1)S(1)}, u32[]{:S(2)}, u32[]{:S(2)}) async-start(bf16[16,64,512]{2,1,0:T(8,128)(2,1)} %broadcast_in_dim.8), calls=%async_computation | async-start | bytes 2097152 | tf_op jit(solution)/shard_map/all_to_all | solution.py:303
  27.4 3.9 %collective-permute-start = (bf16[80,512]{1,0:T(8,128)(2,1)}, bf16[80,512]{1,0:T(8,128)(2,1)}, u32[]{:S(2)}, u32[]{:S(2)}) collective-permute-start(bf16[80,512]{1,0:T(8,128)(2,1)} %fusion.5), channel_id=1, source_target_pairs={{0,8},{8,16},{16,24},{24,32},{32,40},{40,48},{48,56},{56,64},{64,7... | collective-permute-start | bytes 245768 | tf_op jit(solution)/shard_map/ppermute | solution.py:249
  38.5 4.7 %collective-permute-done = bf16[80,512]{1,0:T(8,128)(2,1)} collective-permute-done((bf16[80,512]{1,0:T(8,128)(2,1)}, bf16[80,512]{1,0:T(8,128)(2,1)}, u32[]{:S(2)}, u32[]{:S(2)}) %collective-permute-start) | collective-permute-done | bytes 81952 | tf_op jit(solution)/shard_map/ppermute | solution.py:249
  48.4 3.6 %shard_map.85 = (bf16[2,576,512]{2,1,0:T(8,128)(2,1)S(1)}, bf16[2,592,512]{2,1,0:T(8,128)(2,1)}, f32[2,1,1024]{2,1,0:T(1,128)S(1)}) custom-call(s32[4]{0:T(128)S(1)} %pad_add_fusion.1.index, bf16[2,576,512]{2,1,0:T(8,128)(2,1)S(1)} %pad_maximum_fusion.both, f32[1,512]{1,0:T(1,128)S(1)} %fusion.6.gain, bf16[16,64,512]{2,1,0:T(8,128)(2,1)S(1)} %all-to-all-done.weight), custom_call_target="tpu_custom_call" | custom-call | flops 1207959552 | bytes 1024 | tf_op jit(solution)/shard_map/pallas_call | solution.py:40
  52.0 5.1 %collective-permute-start.23 = (bf16[2,592,512]{2,1,0:T(8,128)(2,1)}, bf16[2,592,512]{2,1,0:T(8,128)(2,1)S(1)}, u32[]{:S(2)}, u32[]{:S(2)}) collective-permute-start(bf16[2,592,512]{2,1,0:T(8,128)(2,1)} %get-tuple-element.95), channel_id=1, source_target_pairs={{0,1},{1,0},{2,3},{3,2},{4,5},{5,4},{6,7},{7,6},{8,9},{9,8},{10,11... | collective-permute-start | bytes 3637256 | tf_op jit(solution)/shard_map/ppermute | solution.py:370
  77.3 17.3 %collective-permute-done.4.crossed = bf16[528,256]{1,0:T(8,128)(2,1)S(1)} collective-permute-done((bf16[528,256]{1,0:T(8,128)(2,1)S(1)}, bf16[528,256]{1,0:T(8,128)(2,1)S(1)}, u32[]{:S(2)}, u32[]{:S(2)}) %collective-permute-start.4) | collective-permute-done | bytes 270368 | tf_op jit(solution)/shard_map/ppermute | solution.py:397
  94.6 2.8 %shard_map.76 = (bf16[512,256]{1,0:T(8,128)(2,1)}, bf16[16,256]{1,0:T(8,128)(2,1)S(1)}) custom-call(bf16[2,512,512]{2,1,0:T(8,128)(2,1)S(1)} %get-tuple-element.65.keep.near, bf16[2,528,512]{2,1,0:T(8,128)(2,1)S(1)} %collective-permute-done.1.core.far, bf16[528,256]{1,0:T(8,128)(2,1)S(1)} %collective-permute-done.2.across, ...), custom_call_target="tpu_custom_call" | custom-call | flops 268435456 | bytes 1024 | tf_op jit(solution)/shard_map/pallas_call | solution.py:40
  97.4 3.1 %shard_map.87 = (bf16[576,256]{1,0:T(8,128)(2,1)}, bf16[16,256]{1,0:T(8,128)(2,1)}) custom-call(bf16[2,576,512]{2,1,0:T(8,128)(2,1)S(1)} %copy-done.1, bf16[2,592,512]{2,1,0:T(8,128)(2,1)S(1)} %collective-permute-done.23.core.far, bf16[592,256]{1,0:T(8,128)(2,1)S(1)} %collective-permute-done.24.across, bf16[592,256]{1,0:T(8,128)(2,1)S(1)} %collective-permute-done.25.flipped, ...), custom_call_target="tpu_custom_call" | custom-call | flops 301989888 | bytes 1024 | tf_op jit(solution)/shard_map/pallas_call | solution.py:40
  107.4 6.6 %collective-permute-done.5.m1 = bf16[512,256]{1,0:T(8,128)(2,1)} collective-permute-done((bf16[512,256]{1,0:T(8,128)(2,1)}, bf16[512,256]{1,0:T(8,128)(2,1)}, u32[]{:S(2)}, u32[]{:S(2)}) %collective-permute-start.5) | collective-permute-done | bytes 262176 | tf_op jit(solution)/shard_map/ppermute | solution.py:410
  116.0 3.2 %slice_bitcast_fusion.1 = (bf16[16,64,512]{2,1,0:T(8,128)(2,1)S(1)}, bf16[16,64,512]{2,1,0:T(8,128)(2,1)S(1)}, bf16[16,64,512]{2,1,0:T(8,128)(2,1)S(1)}, bf16[16...) fusion(bf16[16,8,64,512]{3,2,1,0:T(8,128)(2,1)} %bitcast.74), kind=kLoop, calls=%fused_computation.10 | loop fusion | bytes 10485760 | tf_op jit(solution)/shard_map/squeeze | solution.py:377
  119.2 4.2 %shard_map.88 = (bf16[576,512]{1,0:T(8,128)(2,1)S(1)}, bf16[576,512]{1,0:T(8,128)(2,1)S(1)}, bf16[576,512]{1,0:T(8,128)(2,1)S(1)}, bf16[592,512]{1,0:T(8,128)(2,1)S(1)}, f32[1,1024]{1,0:T(1,128)S(1)}) custom-call(s32[4]{0:T(128)S(1)} %pad_add_fusion.1.index, bf16[576,256]{1,0:T(8,128)(2,1)} %get-tuple-element.102.m0, ...), custom_call_target="tpu_custom_call" | custom-call | flops 2415919104 | bytes 1024 | tf_op jit(solution)/shard_map/pallas_call | solution.py:40
  124.1 3.9 %shard_map.78 = (bf16[512,512]{1,0:T(8,128)(2,1)S(1)}, bf16[512,512]{1,0:T(8,128)(2,1)S(1)}, bf16[512,512]{1,0:T(8,128)(2,1)S(1)}, bf16[528,512]{1,0:T(8,128)(2,1)S(1)}, f32[1,1024]{1,0:T(1,128)S(1)}) custom-call(s32[4]{0:T(128)S(1)} %pad_add_fusion.1.index, bf16[512,256]{1,0:T(8,128)(2,1)} %get-tuple-element.72.m0, ...), custom_call_target="tpu_custom_call" | custom-call | flops 2147483648 | bytes 1024 | tf_op jit(solution)/shard_map/pallas_call | solution.py:40
  131.6 10.7 %collective-permute-done.11.across = bf16[528,256]{1,0:T(8,128)(2,1)S(1)} collective-permute-done((bf16[528,256]{1,0:T(8,128)(2,1)S(1)}, bf16[528,256]{1,0:T(8,128)(2,1)S(1)}, u32[]{:S(2)}, u32[]{:S(2)}) %collective-permute-start.11) | collective-permute-done | bytes 270368 | tf_op jit(solution)/shard_map/ppermute | solution.py:397
  143.5 2.7 %shard_map.90 = (bf16[576,256]{1,0:T(8,128)(2,1)S(1)}, bf16[16,256]{1,0:T(8,128)(2,1)}) custom-call(bf16[576,512]{1,0:T(8,128)(2,1)S(1)} %get-tuple-element.103.keep.near, bf16[592,512]{1,0:T(8,128)(2,1)S(1)} %collective-permute-done.31.core.far, bf16[592,256]{1,0:T(8,128)(2,1)S(1)} %collective-permute-done.32.across, ...), custom_call_target="tpu_custom_call" | custom-call | flops 301989888 | bytes 1024 | tf_op jit(solution)/shard_map/pallas_call | solution.py:40
  149.9 9.0 %collective-permute-done.12.m1 = bf16[512,256]{1,0:T(8,128)(2,1)S(1)} collective-permute-done((bf16[512,256]{1,0:T(8,128)(2,1)S(1)}, bf16[512,256]{1,0:T(8,128)(2,1)S(1)}, u32[]{:S(2)}, u32[]{:S(2)}) %collective-permute-start.12) | collective-permute-done | bytes 262176 | tf_op jit(solution)/shard_map/ppermute | solution.py:410
  163.4 3.5 %shard_map.91 = (bf16[576,512]{1,0:T(8,128)(2,1)S(1)}, bf16[576,512]{1,0:T(8,128)(2,1)S(1)}, bf16[576,512]{1,0:T(8,128)(2,1)S(1)}, bf16[592,512]{1,0:T(8,128)(2,1)S(1)}, f32[1,1024]{1,0:T(1,128)S(1)}) custom-call(s32[4]{0:T(128)S(1)} %pad_add_fusion.1.index, bf16[576,256]{1,0:T(8,128)(2,1)S(1)} %get-tuple-element.109.m0, ...), custom_call_target="tpu_custom_call" | custom-call | flops 2415919104 | bytes 1024 | tf_op jit(solution)/shard_map/pallas_call | solution.py:40
  167.7 3.2 %shard_map.81 = (bf16[512,512]{1,0:T(8,128)(2,1)S(1)}, bf16[512,512]{1,0:T(8,128)(2,1)S(1)}, bf16[512,512]{1,0:T(8,128)(2,1)S(1)}, bf16[528,512]{1,0:T(8,128)(2,1)S(1)}, f32[1,1024]{1,0:T(1,128)S(1)}) custom-call(s32[4]{0:T(128)S(1)} %pad_add_fusion.1.index, bf16[512,256]{1,0:T(8,128)(2,1)S(1)} %get-tuple-element.79.m0, ...), custom_call_target="tpu_custom_call" | custom-call | flops 2147483648 | bytes 1024 | tf_op jit(solution)/shard_map/pallas_call | solution.py:40
  176.2 4.8 %collective-permute-done.17.across = bf16[528,256]{1,0:T(8,128)(2,1)S(1)} collective-permute-done((bf16[528,256]{1,0:T(8,128)(2,1)S(1)}, bf16[528,256]{1,0:T(8,128)(2,1)S(1)}, u32[]{:S(2)}, u32[]{:S(2)}) %collective-permute-start.17) | collective-permute-done | bytes 270368 | tf_op jit(solution)/shard_map/ppermute | solution.py:397
  182.5 5.0 %collective-permute-done.37.across = bf16[592,256]{1,0:T(8,128)(2,1)S(1)} collective-permute-done((bf16[592,256]{1,0:T(8,128)(2,1)S(1)}, bf16[592,256]{1,0:T(8,128)(2,1)S(1)}, u32[]{:S(2)}, u32[]{:S(2)}) %collective-permute-start.37) | collective-permute-done | bytes 303136 | tf_op jit(solution)/shard_map/ppermute | solution.py:397
  195.9 2.9 %collective-permute-done.38.m1 = bf16[576,256]{1,0:T(8,128)(2,1)S(1)} collective-permute-done((bf16[576,256]{1,0:T(8,128)(2,1)S(1)}, bf16[576,256]{1,0:T(8,128)(2,1)S(1)}, u32[]{:S(2)}, u32[]{:S(2)}) %collective-permute-start.38) | collective-permute-done | bytes 294944 | tf_op jit(solution)/shard_map/ppermute | solution.py:410
  207.7 8.4 %collective-permute-done.22 = bf16[448,512]{1,0:T(8,128)(2,1)S(1)} collective-permute-done((bf16[448,512]{1,0:T(8,128)(2,1)S(1)}, bf16[448,512]{1,0:T(8,128)(2,1)S(1)}, u32[]{:S(2)}, u32[]{:S(2)}) %collective-permute-start.22) | collective-permute-done | bytes 458784 | tf_op jit(solution)/shard_map/ppermute | solution.py:436
  216.2 12.5 %collective-permute-done.41 = bf16[576,512]{1,0:T(8,128)(2,1)S(1)} collective-permute-done((bf16[576,512]{1,0:T(8,128)(2,1)S(1)}, bf16[576,512]{1,0:T(8,128)(2,1)S(1)}, u32[]{:S(2)}, u32[]{:S(2)}) %collective-permute-start.41) | collective-permute-done | bytes 589856 | tf_op jit(solution)/shard_map/ppermute | solution.py:436
  (179 shorter events, 85.5 us)
Async XLA Ops:
  6.5 109.4 %all-gather.3.cloned.1.call-start = ((), (), s32[]{:S(2)}) async-start(), calls=%async_computation.1 | async-start | bytes 8912896 | tf_op jit(solution)/shard_map/all_gather | solution.py:335
  18.5 29.9 %all-to-all-start = ((bf16[16,64,512]{2,1,0:T(8,128)(2,1)}), bf16[16,64,512]{2,1,0:T(8,128)(2,1)S(1)}, u32[]{:S(2)}, u32[]{:S(2)}) async-start(bf16[16,64,512]{2,1,0:T(8,128)(2,1)} %broadcast_in_dim.8), calls=%async_computation | async-start | bytes 2097152 | tf_op jit(solution)/shard_map/all_to_all | solution.py:303
  27.4 15.8 %collective-permute-start = (bf16[80,512]{1,0:T(8,128)(2,1)}, bf16[80,512]{1,0:T(8,128)(2,1)}, u32[]{:S(2)}, u32[]{:S(2)}) collective-permute-start(bf16[80,512]{1,0:T(8,128)(2,1)} %fusion.5), channel_id=1, source_target_pairs={{0,8},{8,16},{16,24},{24,32},{32,40},{40,48},{48,56},{56,64},{64,7... | collective-permute-start | bytes 245768 | tf_op jit(solution)/shard_map/ppermute | solution.py:249
  52.0 16.3 %collective-permute-start.23 = (bf16[2,592,512]{2,1,0:T(8,128)(2,1)}, bf16[2,592,512]{2,1,0:T(8,128)(2,1)S(1)}, u32[]{:S(2)}, u32[]{:S(2)}) collective-permute-start(bf16[2,592,512]{2,1,0:T(8,128)(2,1)} %get-tuple-element.95), channel_id=1, source_target_pairs={{0,1},{1,0},{2,3},{3,2},{4,5},{5,4},{6,7},{7,6},{8,9},{9,8},{10,11... | collective-permute-start | bytes 3637256 | tf_op jit(solution)/shard_map/ppermute | solution.py:370
  68.5 29.0 %collective-permute-start.24 = (bf16[592,256]{1,0:T(8,128)(2,1)S(1)}, bf16[592,256]{1,0:T(8,128)(2,1)S(1)}, u32[]{:S(2)}, u32[]{:S(2)}) collective-permute-start(bf16[592,256]{1,0:T(8,128)(2,1)S(1)} %get-tuple-element.97), channel_id=1, source_target_pairs={{0,2},{2,0},{4,6},{6,4},{1,3},{3,1},{5,7},{7,5},{8,10},{10,8},{12,... | collective-permute-start | bytes 909320 | tf_op jit(solution)/shard_map/ppermute | solution.py:397
  69.3 28.1 %collective-permute-start.25 = (bf16[592,256]{1,0:T(8,128)(2,1)S(1)}, bf16[592,256]{1,0:T(8,128)(2,1)S(1)}, u32[]{:S(2)}, u32[]{:S(2)}) collective-permute-start(bf16[592,256]{1,0:T(8,128)(2,1)S(1)} %get-tuple-element.98), channel_id=1, source_target_pairs={{0,6},{2,4},{4,2},{6,0},{1,7},{3,5},{5,3},{7,1},{8,14},{10,12},{12... | collective-permute-start | bytes 909320 | tf_op jit(solution)/shard_map/ppermute | solution.py:397
  69.9 27.5 %collective-permute-start.26 = (bf16[592,256]{1,0:T(8,128)(2,1)S(1)}, bf16[592,256]{1,0:T(8,128)(2,1)S(1)}, u32[]{:S(2)}, u32[]{:S(2)}) collective-permute-start(bf16[592,256]{1,0:T(8,128)(2,1)S(1)} %get-tuple-element.99), channel_id=1, source_target_pairs={{0,4},{2,6},{4,0},{6,2},{1,5},{3,7},{5,1},{7,3},{8,12},{10,14},{12... | collective-permute-start | bytes 909320 | tf_op jit(solution)/shard_map/ppermute | solution.py:397
  73.7 32.7 %collective-permute-start.30 = (bf16[576,512]{1,0:T(8,128)(2,1)}, bf16[576,512]{1,0:T(8,128)(2,1)}, u32[]{:S(2)}, u32[]{:S(2)}) collective-permute-start(bf16[576,512]{1,0:T(8,128)(2,1)} %get-tuple-element.136), channel_id=1, source_target_pairs={{0,6},{2,4},{4,2},{6,0},{1,7},{3,5},{5,3},{7,1},{8,14},{10,12},{12... | collective-permute-start | bytes 1769480 | tf_op jit(solution)/shard_map/ppermute | solution.py:333
  76.2 18.4 %collective-permute-start.4 = (bf16[528,256]{1,0:T(8,128)(2,1)S(1)}, bf16[528,256]{1,0:T(8,128)(2,1)S(1)}, u32[]{:S(2)}, u32[]{:S(2)}) collective-permute-start(bf16[528,256]{1,0:T(8,128)(2,1)S(1)} %get-tuple-element.70), channel_id=1, source_target_pairs={{0,4},{2,6},{4,0},{6,2},{1,5},{3,7},{5,1},{7,3},{8,12},{10,14},{12... | collective-permute-start | bytes 811016 | tf_op jit(solution)/shard_map/ppermute | solution.py:397
  100.6 15.4 %collective-permute-start.27 = (bf16[576,256]{1,0:T(8,128)(2,1)}, bf16[576,256]{1,0:T(8,128)(2,1)S(1)}, u32[]{:S(2)}, u32[]{:S(2)}) collective-permute-start(bf16[576,256]{1,0:T(8,128)(2,1)} %get-tuple-element.102.m0), channel_id=1, source_target_pairs={{0,2},{2,0},{4,6},{6,4},{1,3},{3,1},{5,7},{7,5},{8,10},{10,8},{12,... | collective-permute-start | bytes 884744 | tf_op jit(solution)/shard_map/ppermute | solution.py:410
  100.6 13.4 %collective-permute-start.5 = (bf16[512,256]{1,0:T(8,128)(2,1)}, bf16[512,256]{1,0:T(8,128)(2,1)}, u32[]{:S(2)}, u32[]{:S(2)}) collective-permute-start(bf16[512,256]{1,0:T(8,128)(2,1)} %get-tuple-element.72.m0), channel_id=1, source_target_pairs={{0,2},{2,0},{4,6},{6,4},{1,3},{3,1},{5,7},{7,5},{8,10},{10,8},{12,... | collective-permute-start | bytes 786440 | tf_op jit(solution)/shard_map/ppermute | solution.py:410
  102.8 21.3 %collective-permute-start.8 = (bf16[512,512]{1,0:T(8,128)(2,1)}, bf16[512,512]{1,0:T(8,128)(2,1)S(1)}, u32[]{:S(2)}, u32[]{:S(2)}) collective-permute-start(bf16[512,512]{1,0:T(8,128)(2,1)} %get-tuple-element.142), channel_id=1, source_target_pairs={{0,6},{2,4},{4,2},{6,0},{1,7},{3,5},{5,3},{7,1},{8,14},{10,12},{12... | collective-permute-start | bytes 1572872 | tf_op jit(solution)/shard_map/ppermute | solution.py:333
  103.1 21.0 %collective-permute-start.6 = (bf16[512,256]{1,0:T(8,128)(2,1)}, bf16[512,256]{1,0:T(8,128)(2,1)}, u32[]{:S(2)}, u32[]{:S(2)}) collective-permute-start(bf16[512,256]{1,0:T(8,128)(2,1)} %get-tuple-element.72.m0), channel_id=1, source_target_pairs={{0,1},{1,0},{2,3},{3,2},{4,5},{5,4},{6,7},{7,6},{8,9},{9,8},{10,11... | collective-permute-start | bytes 786440 | tf_op jit(solution)/shard_map/ppermute | solution.py:409
  106.4 12.8 %collective-permute-start.28 = (bf16[576,256]{1,0:T(8,128)(2,1)}, bf16[576,256]{1,0:T(8,128)(2,1)S(1)}, u32[]{:S(2)}, u32[]{:S(2)}) collective-permute-start(bf16[576,256]{1,0:T(8,128)(2,1)} %get-tuple-element.102.m0), channel_id=1, source_target_pairs={{0,1},{1,0},{2,3},{3,2},{4,5},{5,4},{6,7},{7,6},{8,9},{9,8},{10,11... | collective-permute-start | bytes 884744 | tf_op jit(solution)/shard_map/ppermute | solution.py:409
  128.1 35.3 %collective-permute-start.15 = (bf16[16,64,512]{2,1,0:T(8,128)(2,1)S(1)}, bf16[16,64,512]{2,1,0:T(8,128)(2,1)S(1)}, u32[]{:S(2)}, u32[]{:S(2)}) collective-permute-start(bf16[16,64,512]{2,1,0:T(8,128)(2,1)S(1)} %get-tuple-element.128.w2), channel_id=1, source_target_pairs={{0,6},{2,4},{4,2},{6,0},{1,7},{3,5},{5,3},{7,1},{8,14},{10,12},{12... | collective-permute-start | bytes 3145736 | tf_op jit(solution)/shard_map/ppermute | solution.py:378
  128.4 15.0 %collective-permute-start.32 = (bf16[592,256]{1,0:T(8,128)(2,1)S(1)}, bf16[592,256]{1,0:T(8,128)(2,1)S(1)}, u32[]{:S(2)}, u32[]{:S(2)}) collective-permute-start(bf16[592,256]{1,0:T(8,128)(2,1)S(1)} %get-tuple-element.106), channel_id=1, source_target_pairs={{0,2},{2,0},{4,6},{6,4},{1,3},{3,1},{5,7},{7,5},{8,10},{10,8},{12,... | collective-permute-start | bytes 909320 | tf_op jit(solution)/shard_map/ppermute | solution.py:397
  146.2 15.0 %collective-permute-start.33 = (bf16[576,256]{1,0:T(8,128)(2,1)S(1)}, bf16[576,256]{1,0:T(8,128)(2,1)S(1)}, u32[]{:S(2)}, u32[]{:S(2)}) collective-permute-start(bf16[576,256]{1,0:T(8,128)(2,1)S(1)} %get-tuple-element.109.m0), channel_id=1, source_target_pairs={{0,2},{2,0},{4,6},{6,4},{1,3},{3,1},{5,7},{7,5},{8,10},{10,8},{12,... | collective-permute-start | bytes 884744 | tf_op jit(solution)/shard_map/ppermute | solution.py:410
  146.5 12.3 %collective-permute-start.12 = (bf16[512,256]{1,0:T(8,128)(2,1)S(1)}, bf16[512,256]{1,0:T(8,128)(2,1)S(1)}, u32[]{:S(2)}, u32[]{:S(2)}) collective-permute-start(bf16[512,256]{1,0:T(8,128)(2,1)S(1)} %get-tuple-element.79.m0), channel_id=1, source_target_pairs={{0,2},{2,0},{4,6},{6,4},{1,3},{3,1},{5,7},{7,5},{8,10},{10,8},{12,... | collective-permute-start | bytes 786440 | tf_op jit(solution)/shard_map/ppermute | solution.py:410
  147.7 20.0 %collective-permute-start.13 = (bf16[512,256]{1,0:T(8,128)(2,1)S(1)}, bf16[512,256]{1,0:T(8,128)(2,1)S(1)}, u32[]{:S(2)}, u32[]{:S(2)}) collective-permute-start(bf16[512,256]{1,0:T(8,128)(2,1)S(1)} %get-tuple-element.79.m0), channel_id=1, source_target_pairs={{0,1},{1,0},{2,3},{3,2},{4,5},{5,4},{6,7},{7,6},{8,9},{9,8},{10,11... | collective-permute-start | bytes 786440 | tf_op jit(solution)/shard_map/ppermute | solution.py:409
  149.8 13.5 %collective-permute-start.34 = (bf16[576,256]{1,0:T(8,128)(2,1)S(1)}, bf16[576,256]{1,0:T(8,128)(2,1)S(1)}, u32[]{:S(2)}, u32[]{:S(2)}) collective-permute-start(bf16[576,256]{1,0:T(8,128)(2,1)S(1)} %get-tuple-element.109.m0), channel_id=1, source_target_pairs={{0,1},{1,0},{2,3},{3,2},{4,5},{5,4},{6,7},{7,6},{8,9},{9,8},{10,11... | collective-permute-start | bytes 884744 | tf_op jit(solution)/shard_map/ppermute | solution.py:409
  171.0 30.0 %collective-permute-start.21 = (bf16[16,64,512]{2,1,0:T(8,128)(2,1)S(1)}, bf16[16,64,512]{2,1,0:T(8,128)(2,1)S(1)}, u32[]{:S(2)}, u32[]{:S(2)}) collective-permute-start(bf16[16,64,512]{2,1,0:T(8,128)(2,1)S(1)} %get-tuple-element.125.w0), channel_id=1, source_target_pairs={{0,6},{2,4},{4,2},{6,0},{1,7},{3,5},{5,3},{7,1},{8,14},{10,12},{12... | collective-permute-start | bytes 3145736 | tf_op jit(solution)/shard_map/ppermute | solution.py:434
  173.8 13.7 %collective-permute-start.37 = (bf16[592,256]{1,0:T(8,128)(2,1)S(1)}, bf16[592,256]{1,0:T(8,128)(2,1)S(1)}, u32[]{:S(2)}, u32[]{:S(2)}) collective-permute-start(bf16[592,256]{1,0:T(8,128)(2,1)S(1)} %get-tuple-element.115), channel_id=1, source_target_pairs={{0,2},{2,0},{4,6},{6,4},{1,3},{3,1},{5,7},{7,5},{8,10},{10,8},{12,... | collective-permute-start | bytes 909320 | tf_op jit(solution)/shard_map/ppermute | solution.py:397
  202.7 13.4 %collective-permute-start.22 = (bf16[448,512]{1,0:T(8,128)(2,1)S(1)}, bf16[448,512]{1,0:T(8,128)(2,1)S(1)}, u32[]{:S(2)}, u32[]{:S(2)}) collective-permute-start(bf16[448,512]{1,0:T(8,128)(2,1)S(1)} %get-tuple-element.93), channel_id=1, source_target_pairs={{0,6},{2,4},{4,2},{6,0},{1,7},{3,5},{5,3},{7,1},{8,14},{10,12},{12... | collective-permute-start | bytes 1376264 | tf_op jit(solution)/shard_map/ppermute | solution.py:436
  206.6 22.1 %collective-permute-start.41 = (bf16[576,512]{1,0:T(8,128)(2,1)S(1)}, bf16[576,512]{1,0:T(8,128)(2,1)S(1)}, u32[]{:S(2)}, u32[]{:S(2)}) collective-permute-start(bf16[576,512]{1,0:T(8,128)(2,1)S(1)} %get-tuple-element.122), channel_id=1, source_target_pairs={{0,6},{2,4},{4,2},{6,0},{1,7},{3,5},{5,3},{7,1},{8,14},{10,12},{12... | collective-permute-start | bytes 1769480 | tf_op jit(solution)/shard_map/ppermute | solution.py:436
  (38 other events, 279.9 us)
Sparse Core Ops, SparseCore 0:
  17.5 79.5 all-gather.2
